TPU v7x, 512 devices: a whole 4x8x8 slice. The times are simulated.
512 devices in a mesh: sp: 64 (over z, y), fs: 4 (over x), tp: 2 (over core).
Axes of the slice: x: 4, y: 8, z: 8, core: 2. Of those that a mesh axis runs over, the one named last changes fastest.
Arguments:
- tokens: bfloat16 [12288, 4096], P('sp', ('fs', 'tp')), may hold values from -6 to 6
- norm_gain: float32 [4096], replicated, may hold values from 0.1 to 1.9
- w_conv_in: bfloat16 [4096, 1024], P('sp', ('fs', 'tp')), may hold values from -0.09375 to 0.09375
- w_conv_b: bfloat16 [4096, 1024], P('sp', ('fs', 'tp')), may hold values from -0.09375 to 0.09375
- w_conv_c: bfloat16 [4096, 1024], P('sp', ('fs', 'tp')), may hold values from -0.09375 to 0.09375
- conv_taps: float32 [3, 1024], P(None, ('fs', 'tp')), may hold values from -1.2 to 1.2
- w_query: bfloat16 [4096, 2048], P('sp', ('fs', 'tp')), may hold values from -1 to 1
- w_key: bfloat16 [4096, 2048], P('sp', ('fs', 'tp')), may hold values from -1 to 1
- w_value: bfloat16 [4096, 2048], P('sp', ('fs', 'tp')), may hold values from -0.09375 to 0.09375
- lam: float32 [8], P(('fs', 'tp')), may hold values from 0.3 to 0.8
- head_scale: float32 [8, 256], P(('fs', 'tp')), may hold values from 0.2 to 3.5
- gain_conv: float32 [1024], P(('fs', 'tp')), may hold values from 0.1 to 1.9
- gain_attn: float32 [2048], P(('fs', 'tp')), may hold values from 0.1 to 1.9
Outputs:
- conv_mixed: float32 [12288, 1024], P('sp', ('fs', 'tp'))
- attn_mixed: float32 [12288, 2048], P('sp', ('fs', 'tp'))
All inputs are finite; a program needn't handle non-finite values.
Results may differ from a plain program's by a relative error of at most 0.012.
The roundings to bfloat16 on the way count: a program that leaves them out, or rounds other values in their place, can miss the bound.
Values may be sent and summed in bfloat16 or wider, within the bound.
A program may use at most 128 MiB of HBM per device.

v0:
```python
import jax
import jax.numpy as jnp
from jax import lax
from jax.sharding import PartitionSpec as P

CH = 1024
HEADS = 8
DV = 256
BLOCK = 64


EPS = 1e-06
masked_score = -1e30


def from_everyone(array, axis):
    copies = jnp.broadcast_to(array, (lax.axis_size(axis), *array.shape))
    return lax.all_to_all(copies, axis, split_axis=0, concat_axis=0, tiled=True)


def in_order(pieces, dim):
    pieces = jnp.moveaxis(pieces, 0, dim)
    dims = pieces.shape
    return pieces.reshape(*dims[:dim], dims[dim] * dims[dim + 1], *dims[dim + 2 :])


def collect(array, axis, dim):
    pieces = from_everyone(array, axis)
    return in_order(pieces, dim)


def side_by_side(arrays, axis, dim, along):
    widths = [a.shape[along] for a in arrays]
    both = jnp.concatenate(arrays, axis=along)
    result = lax.all_gather(both, axis, axis=dim, tiled=True)
    return tuple(jnp.split(result, [sum(widths[:k]) for k in range(1, len(widths))], axis=along))


def from_behind(block, axis, distance):
    devices = range(lax.axis_size(axis))
    route = [(i - distance, i) for i in devices if i - distance in devices]
    return lax.ppermute(block, axis, route)


def in_one_piece(arrays, axis, dim, along):
    columns = [a.reshape(*a.shape[:along], -1) for a in arrays]
    both = jnp.concatenate(columns, axis=along)
    result, at, gathered = (lax.all_gather(both, axis, axis=dim, tiled=True), 0, [])
    for a, column in zip(arrays, columns):
        piece = result[..., at : at + column.shape[along]]
        gathered.append(piece.reshape(*piece.shape[:along], *a.shape[along:]))
        at += column.shape[along]
    return tuple(gathered)


def of_everyone(array, axis):
    return from_everyone(array, axis).sum(axis=0)


def make_absorber(normed):

    def absorb_rows(running, pieces, start):
        return tuple(
            (jnp.dot(normed, piece, preferred_element_type=jnp.float32) for piece in pieces)
        )

    return absorb_rows


def absorb_keys(carried, queries, key_rows, value_rows, visible):
    row_max, row_total, accumulated = carried
    scores = jnp.einsum(
        "qhcd,khcd->chqk", queries, key_rows, preferred_element_type=jnp.float32
    ) * queries.shape[3] ** (-0.5)
    mask_full = visible[None, None]
    scores = jnp.where(mask_full, scores, masked_score)
    new_max = jnp.maximum(row_max, jnp.max(scores, axis=-1))
    weights = jnp.where(mask_full, jnp.exp(scores - new_max[..., None]), 0.0)
    row_total = jnp.sum(weights, axis=-1)
    product = jnp.einsum(
        "chqk,khd->chqd",
        weights.astype(jnp.bfloat16),
        value_rows,
        preferred_element_type=jnp.float32,
    )
    accumulated = product
    return (new_max, row_total, accumulated)


def blank_sum(tok_rows, weight):
    return jnp.zeros((tok_rows, weight.shape[1]), jnp.float32)


def local(
    tokens,
    norm_gain,
    w_conv_in,
    w_conv_b,
    w_conv_c,
    conv_taps,
    w_query,
    w_key,
    w_value,
    lam,
    head_scale,
    gain_conv,
    gain_attn,
):
    gathered = collect(tokens, ("fs", "tp"), 1)
    as_float = gathered.astype(jnp.float32)
    normed = (
        as_float
        * lax.rsqrt(jnp.mean(as_float * as_float, axis=-1, keepdims=True) + EPS)
        * norm_gain
    ).astype(jnp.bfloat16)
    tok_rows = normed.shape[0]
    absorb_rows = make_absorber(normed)
    conv_in, conv_b, conv_c, query_sum, key_sum, value_sum = absorb_rows(
        (
            blank_sum(tok_rows, w_conv_in),
            blank_sum(tok_rows, w_conv_b),
            blank_sum(tok_rows, w_conv_c),
            blank_sum(tok_rows, w_query),
            blank_sum(tok_rows, w_key),
            blank_sum(tok_rows, w_value),
        ),
        side_by_side((w_conv_in, w_conv_b, w_conv_c, w_query, w_key, w_value), "sp", 0, 1),
        jnp.int32(0),
    )
    seq_rank = lax.axis_index("sp")
    conv_in = conv_in.astype(jnp.bfloat16)
    conv_b = conv_b.astype(jnp.bfloat16)
    conv_c = conv_c.astype(jnp.bfloat16)
    mixed_in = (conv_c.astype(jnp.float32) * conv_in.astype(jnp.float32)).astype(jnp.bfloat16)
    earlier = from_behind(mixed_in[-2:], "sp", 1)
    earlier = jnp.where(seq_rank > 0, earlier, jnp.zeros_like(earlier))
    padded = jnp.concatenate([earlier, mixed_in], axis=0).astype(jnp.float32)
    convolved = conv_taps[0] * padded[:-2] + conv_taps[1] * padded[1:-1] + conv_taps[2] * padded[2:]
    conv_out = conv_b.astype(jnp.float32) * convolved
    heads_here = lam.shape[0]
    queries = query_sum.astype(jnp.bfloat16).reshape(tok_rows, heads_here, 2, -1)
    key_rows = key_sum.astype(jnp.bfloat16).reshape(tok_rows, heads_here, 2, -1)
    value_rows = value_sum.astype(jnp.bfloat16).reshape(tok_rows, heads_here, -1)
    value_width = value_rows.shape[2]
    positions = jnp.arange(tok_rows)
    query_blocks = (seq_rank * tok_rows + positions) // BLOCK
    carried = (
        jnp.full((2, heads_here, tok_rows), masked_score, jnp.float32),
        jnp.zeros((2, heads_here, tok_rows), jnp.float32),
        jnp.zeros((2, heads_here, tok_rows, value_width), jnp.float32),
    )
    pieces = in_one_piece((key_rows, value_rows), "sp", 0, 2)
    key_blocks = jnp.arange(pieces[0].shape[0]) // BLOCK
    visible = key_blocks[None, :] <= query_blocks[:, None]
    carried = absorb_keys(carried, queries, pieces[0], pieces[1], visible)
    row_max, row_total, accumulated = carried
    readout = accumulated / row_total[..., None]
    difference = readout[0] - lam[:, None, None] * readout[1]
    headed = (
        difference
        * lax.rsqrt(jnp.mean(difference * difference, axis=-1, keepdims=True) + EPS)
        * head_scale[:, None, :]
    )
    attn = headed.transpose(1, 0, 2).reshape(tok_rows, heads_here * value_width)
    squares = jnp.sum(conv_out * conv_out, axis=1) + jnp.sum(attn * attn, axis=1)
    total = of_everyone(squares, ("fs", "tp"))
    inv_rms = lax.rsqrt(total / (CH + HEADS * DV) + EPS)[:, None]
    conv_mixed = conv_out * inv_rms * gain_conv
    attn_mixed = attn * inv_rms * gain_attn
    return (conv_mixed, attn_mixed)


def solution(mesh):
    in_specs = (
        P("sp", ("fs", "tp")),
        P(),
        P("sp", ("fs", "tp")),
        P("sp", ("fs", "tp")),
        P("sp", ("fs", "tp")),
        P(None, ("fs", "tp")),
        P("sp", ("fs", "tp")),
        P("sp", ("fs", "tp")),
        P("sp", ("fs", "tp")),
        P(("fs", "tp")),
        P(("fs", "tp"), None),
        P(("fs", "tp")),
        P(("fs", "tp")),
    )
    out_specs = (P("sp", ("fs", "tp")), P("sp", ("fs", "tp")))
    return jax.shard_map(local, mesh=mesh, in_specs=in_specs, out_specs=out_specs, check_vma=False)
```

profile of v0, /device:TPU:1, one launch (start us, length us, event | category | flops | bytes accessed | tf_op | source)
XLA Modules:
  0.0 309.3 jit_solution(13268219771968465351)
XLA Ops:
  7.2 0.0 all-gather.3.cloned.1.call-start
  7.2 0.7 constant_dynamic-update-slice_fusion.5
  7.9 0.7 constant_dynamic-update-slice_fusion.4
  8.7 0.7 constant_dynamic-update-slice_fusion.3
  9.4 0.8 constant_dynamic-update-slice_fusion.2
  10.1 0.8 constant_dynamic-update-slice_fusion.1
  10.9 0.8 constant_dynamic-update-slice_fusion
  11.7 0.7 copy-done.2
  12.3 0.0 all-gather.3.cloned.1.call-update
  12.4 0.0 all-gather.5.cloned.1.call-start
  12.4 1.1 broadcast_in_dim.43
  13.5 29.8 %all_to_all.11 = bf16[8,192,512]{2,1,0:T(8,128)(2,1)S(1)} all-to-all(bf16[8,192,512]{2,1,0:T(8,128)(2,1)S(1)} %broadcast_in_dim.43), channel_id=1, replica_groups=mesh['sp'=64,'fs'=4,'tp'=2] {'fs','tp'}, dimensions={0} | all-to-all | bytes 3145728 | tf_op jit(solution)/shard_map/all_to_all | solution.py:18
  43.3 0.4 convert_bitcast_fusion
  43.7 0.0 copy-start.3
  43.7 0.4 copy.31
  44.2 0.4 fusion.8
  44.6 0.0 copy-done.3
  44.6 0.4 multiply_convert_fusion
  45.0 0.0 copy-start
  45.0 0.0 copy-start.5
  45.0 76.8 %all-gather.3.cloned.1.call-done = bf16[4096,1152]{1,0:T(8,128)(2,1)} async-done(((bf16[64,1152]{1,0:T(8,128)(2,1)}), bf16[4096,1152]{1,0:T(8,128)(2,1)}) %all-gather.3.cloned.1.call-update) | async-done | bytes 9437200 | tf_op jit(solution)/shard_map/all_gather | solution.py:35
  121.9 2.2 fusion.30
  124.0 2.2 fusion.33
  126.2 0.7 pad_maximum_fusion
  126.9 0.0 copy-done
  126.9 0.0 all-gather.5.cloned.1.call-update
  127.7 0.0 copy-done.5
  127.8 1.4 broadcast_compare_fusion
  129.2 2.3 fusion.39
  131.4 1.8 fusion.38
  133.2 3.3 %collective-permute-start = (bf16[2,128]{1,0:T(2,128)(2,1)S(1)}, bf16[2,128]{1,0:T(2,128)(2,1)S(1)}, u32[]{:S(2)}, u32[]{:S(2)}) collective-permute-start(bf16[2,128]{1,0:T(2,128)(2,1)S(1)} %slice.44), channel_id=1, source_target_pairs={{0,8},{8,16},{16,24},{24,32},{32,40},{40,48},{48,56},{56,64},{64,7... | collective-permute-start | bytes 1544 | tf_op jit(solution)/shard_map/ppermute | solution.py:42
  136.5 2.2 fusion.27
  138.7 0.0 collective-permute-done
  138.8 1.9 multiply_reduce_fusion.2
  140.7 103.8 %all-gather.5.cloned.1.call-done = bf16[12288,1,512]{2,0,1:T(8,128)(2,1)} async-done(((bf16[192,1,512]{2,0,1:T(8,128)(2,1)}), bf16[12288,1,512]{2,0,1:T(8,128)(2,1)}) %all-gather.5.cloned.1.call-update) | async-done | bytes 12582928 | tf_op jit(solution)/shard_map/all_gather | solution.py:48
  244.5 6.4 %slice.49 = bf16[12288,1,256]{2,0,1:T(8,128)(2,1)} slice(bf16[12288,1,512]{2,0,1:T(8,128)(2,1)} %all-gather.5.cloned.1.call-done), slice={[0:12288], [0:1], [0:256]} | slice | bytes 12582912 | tf_op jit(solution)/shard_map/slice | solution.py:50
  251.0 9.7 %reshape.207 = bf16[12288,2,128]{2,1,0:T(2,128)(2,1)} reshape(bf16[12288,1,256]{2,0,1:T(8,128)(2,1)} %slice.49) | data formatting | bytes 12582912 | tf_op jit(solution)/shard_map/reshape.3
  260.7 11.4 %fusion.62 = (f32[2,192]{1,0:T(2,128)S(1)}, f32[2,192,12288]{2,1,0:T(8,128)}) fusion(bf16[12288,2,128]{2,1,0:T(2,128)(2,1)} %reshape.207, bf16[24,2,8,128]{3,2,1,0:T(8,128)(2,1)S(1)} %fusion.27, pred[192,12288]{1,0:T(8,128)(4,1)S(1)} %broadcast_compare_fusion), kind=kOutput, calls=%fused_computation.86 | convolution fusion | flops 1222114944 | bytes 27624960 | tf_op jit(solution)/shard_map/qhcd,khcd->chqk/dot_general | solution.py:72
  272.1 8.9 %fusion = f32[2,192]{1,0:T(2,128)S(1)} fusion(f32[2,192,12288]{2,1,0:T(8,128)} %get-tuple-element.10, f32[2,192]{1,0:T(2,128)S(1)} %broadcast_maximum_fusion, pred[192,12288]{1,0:T(8,128)(4,1)S(1)} %broadcast_compare_fusion), kind=kLoop, calls=%fused_computation.2 | loop fusion | flops 14155392 | bytes 21236736 | tf_op jit(solution)/shard_map/reduce_sum | solution.py:79
  281.0 0.0 copy-start.4
  281.0 0.0 copy-start.6
  281.0 0.0 copy-start.7
  281.0 10.0 %fusion.48 = f32[2,1,192,256]{3,2,0,1:T(8,128)S(1)} fusion(f32[2,192,12288]{2,1,0:T(8,128)} %get-tuple-element.10, f32[2,192]{1,0:T(2,128)S(1)} %broadcast_maximum_fusion, pred[192,12288]{1,0:T(8,128)(4,1)S(1)} %broadcast_compare_fusion, bf16[12288,1,512]{2,0,1:T(8,128)(2,1)} %all-gather.5.cloned.1.call-done, f32[2,192]{1,0:T(2,128)S(1)} %fusion), kind=kOutput, calls=%fused_computation.41 | convolution fusion | flops 2430173184 | bytes 27921408 | tf_op jit(solution)/shard_map/chqk,khd->chqd/dot_general | solution.py:80
  291.1 0.1 multiply_reduce_fusion.1
  291.2 0.2 multiply_reduce_fusion
  291.4 9.5 %all_to_all.12 = f32[8,1,192]{2,1,0:T(1,128)S(1)} all-to-all(f32[8,1,192]{2,1,0:T(1,128)S(1)} %broadcast_in_dim.49), channel_id=1, replica_groups=mesh['sp'=64,'fs'=4,'tp'=2] {'fs','tp'}, dimensions={0} | all-to-all | bytes 12288 | tf_op jit(solution)/shard_map/all_to_all | solution.py:18
  301.0 0.8 multiply_multiply_fusion
  301.8 0.7 multiply_multiply_fusion.1
  (19 shorter events, 0.1 us)
Async XLA Ops:
  7.2 114.7 %all-gather.3.cloned.1.call-start = ((), (), s32[]{:S(2)}) async-start(), calls=%async_computation.2 | async-start | bytes 9584640 | tf_op jit(solution)/shard_map/all_gather | solution.py:35
  11.7 0.7 copy-start.2
  12.4 232.2 %all-gather.5.cloned.1.call-start = ((), (), s32[]{:S(2)}) async-start(), calls=%async_computation.3 | async-start | bytes 12779520 | tf_op jit(solution)/shard_map/all_gather | solution.py:48
  43.7 0.9 copy-start.3
  45.0 81.9 %copy-start = (bf16[192,4096]{1,0:T(8,128)(2,1)}, bf16[192,4096]{1,0:T(8,128)(2,1)S(1)}, u32[]{:S(2)}) copy-start(bf16[192,4096]{1,0:T(8,128)(2,1)S(1)} %multiply_convert_fusion) | copy-start | bytes 4718596
  45.0 82.7 %copy-start.5 = (f32[3,128]{1,0:T(4,128)S(1)}, f32[3,128]{1,0:T(4,128)}, u32[]{:S(2)}) copy-start(f32[3,128]{1,0:T(4,128)} %param.18) | copy-start | bytes 4612
  126.9 4.5 %copy-start.1 = (bf16[192,4096]{1,0:T(8,128)(2,1)S(1)}, bf16[192,4096]{1,0:T(8,128)(2,1)}, u32[]{:S(2)}) copy-start(bf16[192,4096]{1,0:T(8,128)(2,1)} %copy-done) | copy-start | bytes 4718596
  133.2 5.5 %collective-permute-start = (bf16[2,128]{1,0:T(2,128)(2,1)S(1)}, bf16[2,128]{1,0:T(2,128)(2,1)S(1)}, u32[]{:S(2)}, u32[]{:S(2)}) collective-permute-start(bf16[2,128]{1,0:T(2,128)(2,1)S(1)} %slice.44), channel_id=1, source_target_pairs={{0,8},{8,16},{16,24},{24,32},{32,40},{40,48},{48,56},{56,64},{64,7... | collective-permute-start | bytes 1544 | tf_op jit(solution)/shard_map/ppermute | solution.py:42
  281.0 10.2 %copy-start.4 = (f32[1,256]{1,0:T(1,128)S(1)}, f32[1,256]{1,0:T(1,128)}, u32[]{:S(2)}) copy-start(f32[1,256]{1,0:T(1,128)} %param.23) | copy-start | bytes 3076
  281.0 19.9 %copy-start.6 = (f32[256]{0:T(256)S(1)}, f32[256]{0:T(256)}, u32[]{:S(2)}) copy-start(f32[256]{0:T(256)} %param.25) | copy-start | bytes 3076
  281.0 20.7 %copy-start.7 = (f32[128]{0:T(128)S(1)}, f32[128]{0:T(128)}, u32[]{:S(2)}) copy-start(f32[128]{0:T(128)} %param.24) | copy-start | bytes 1540
Sparse Core Ops, SparseCore 0:
  12.5 109.3 all-gather.2
  127.1 117.4 all-gather.4
where the time goes:
time: 310 us; the launch traced here: 309 us
  waiting for transfers between devices  181 us (58%)
  blocking collectives  39.3 us (13%)
  matrix products  33.9 us (11%)
  local copies, waits for them, and re-layouts  22.8 us (7%)
  between operations  15.1 us (5%)
  other arithmetic  14.2 us (5%)
  starting transfers between devices  3.37 us (1%)
    all_gather x1, waiting for transfers between devices, in_one_piece(): lax.all_gather(both, axis, axis=dim, tiled=True)  104 us
    all_gather x1, waiting for transfers between devices, side_by_side(): result = lax.all_gather(both, axis, axis=dim, tiled=True)  76.8 us
    all_to_all x2, blocking collectives, from_everyone(): return lax.all_to_all(copies, axis, split_axis=0, concat_axis=0, tiled=True)  39.3 us
    dot_general x6, matrix products, absorb_rows(): jnp.dot(normed, piece, preferred_element_type=jnp.float32)  12.5 us
    dot_general x1, matrix products, absorb_keys(): jnp.einsum('qhcd,khcd->chqk', queries, key_rows, preferred_element_type=j...  11.4 us
    dot_general x1, matrix products, absorb_keys(): jnp.einsum('chqk,khd->chqd', weights.astype(jnp.bfloat16), value_rows, pr...  10 us
    another operation x1, local copies, waits for them, and re-layouts  9.72 us
    reduce_sum x1, other arithmetic, absorb_keys(): row_total = jnp.sum(weights, axis=-1)  8.9 us
  transfers between devices with their start and end apart: 3, of which 2 were waited for; matrix products, arithmetic and copies ran while one was open for 4% of the time, Pallas kernels for 0%

commit v1 on v0

v1 whole, which is shorter than its diff:
```python
import functools
import math

import jax
import jax.numpy as jnp
from jax import lax
from jax.experimental import pallas as pl
from jax.experimental.pallas import tpu as pltpu
from jax.sharding import PartitionSpec as P

NY = 8
NZ = 8
D = 4096
CH = 1024
HEADS = 8
DK = 128
DV = 256
ROWS = 192
UNIT = 64
EPS = 1e-06
MASKED = -1e30
LOG2E = 1.4426950408889634
LN2 = 0.6931471805599453
MESH = pl.DeviceIdType.MESH

COLS = 1152
PIECES = ((0, 256), (256, 256), (512, 256), (768, 384))


def rem(a, n):
    return lax.rem(a, jnp.int32(n))


def div(a, n):
    return lax.div(a, jnp.int32(n))


def to_row(column):
    wide = jnp.broadcast_to(column, (ROWS, 128))
    return jnp.transpose(wide)[0:8]


def to_column(row):
    tall = jnp.broadcast_to(row, (128, ROWS))
    return jnp.transpose(tall)[:, 0:1]


def kernel(
    tokens,
    w_key,
    w_value,
    w_query,
    w_conv_in,
    w_conv_b,
    w_conv_c,
    norm_gain,
    conv_taps,
    lam,
    head_scale,
    gain_conv,
    gain_attn,
    conv_ref,
    attn_ref,
    tok,
    wts,
    nrm,
    acc,
    keys,
    values,
    queries,
    mixed,
    halo,
    out_slots,
    out_rows,
    in_slots,
    in_rows,
    squares,
    conv_out,
    read,
    local_sem,
    tok_send,
    tok_recv,
    w_send,
    w_recv,
    k_send,
    k_recv,
    v_send,
    v_recv,
    q_send,
    q_recv,
    halo_send,
    halo_recv,
    o_send,
    o_recv,
    l_send,
    l_recv,
    s_send,
    s_recv,
):
    sp = lax.axis_index("sp")
    x = lax.axis_index("fs")
    core = lax.axis_index("tp")
    y = rem(sp, NY)
    z = div(sp, NY)
    mine = 2 * x + core

    def at(s, f=x, t=core):
        return (s, f, t)

    def along_y(d):
        return sp + rem(y + d + NY, NY) - y

    def along_z(d):
        return sp + (rem(z + d + NZ, NZ) - z) * NY

    def send(src, dst, send_sem, recv_sem, device):
        pltpu.make_async_remote_copy(
            src_ref=src,
            dst_ref=dst,
            send_sem=send_sem,
            recv_sem=recv_sem,
            device_id=device,
            device_id_type=MESH,
        ).start()

    def arrived(ref, sem):
        pltpu.make_async_copy(ref, ref, sem).wait()

    own = [
        pltpu.make_async_copy(tokens, tok.at[mine], local_sem.at[0]),
    ]
    start = 0
    for k, w in enumerate((w_key, w_value, w_query, w_conv_in, w_conv_b, w_conv_c)):
        width = w.shape[1]
        own.append(
            pltpu.make_async_copy(
                w, wts.at[sp, :, pl.ds(start, width)], local_sem.at[1 + k]
            )
        )
        start += width
    for copy in own:
        copy.start()

    barrier = pltpu.get_barrier_semaphore()

    def greet(device):
        pl.semaphore_signal(barrier, inc=1, device_id=device, device_id_type=MESH)

    for d in (1, -1):
        greet(at(along_y(d)))
        greet(at(along_z(d)))
    for k in range(1, 8):
        other = rem(mine + k, 8)
        greet((sp, div(other, 2), rem(other, 2)))
    before = rem(sp + NY * NZ - 1, NY * NZ)
    after = rem(sp + 1, NY * NZ)
    greet(at(before))
    for copy in own:
        copy.wait()
    pl.semaphore_wait(barrier, 12)

    for k in (1, 3, 2):
        send(
            tok.at[mine],
            tok.at[mine],
            tok_send,
            tok_recv.at[mine],
            at(sp, rem(x + k, 4)),
        )
    send(tok.at[mine], tok.at[mine], tok_send, tok_recv.at[mine], at(sp, x, 1 - core))

    stride1 = 1 + 7 * core
    stride2 = 8 - 7 * core
    pos1 = rem(lax.div(sp, stride1), 8)
    pos2 = rem(lax.div(sp, stride2), 8)

    def unit(d1, d2):
        return rem(pos1 + d1 + 8, 8) * stride1 + rem(pos2 + d2 + 8, 8) * stride2

    def pass_on(u, d1, d2):
        send(wts.at[u], wts.at[u], w_send, w_recv.at[u], at(unit(d1, d2)))

    def w_wait(u):
        arrived(wts.at[u], w_recv.at[u])

    def offset(j):
        return div(j + 1, 2) * (1 - 2 * rem(j, 2))

    def multiply(u):
        rows = nrm[u]
        for first, width in PIECES:
            cols = pl.ds(first, width)
            acc[:, cols] += jnp.dot(
                rows, wts[u, :, cols], preferred_element_type=jnp.float32
            )

    def first_ring(j, _):
        off = offset(j)
        u = unit(off, 0)

        @pl.when(j > 0)
        def _():
            w_wait(u)

        @pl.when(jnp.logical_and(off <= 0, off > -4))
        def _():
            pass_on(u, 1, 0)

        @pl.when(jnp.logical_and(off >= 0, off < 3))
        def _():
            pass_on(u, -1, 0)

        pass_on(u, 0, 1)
        pass_on(u, 0, -1)
        return 0

    lax.fori_loop(0, 3, first_ring, 0)
    for k in (1, 3, 2):
        slot = 2 * rem(x + k, 4) + core
        arrived(tok.at[slot], tok_recv.at[slot])
        send(tok.at[slot], tok.at[slot], tok_send, tok_recv.at[slot], at(sp, x, 1 - core))
    lax.fori_loop(3, 8, first_ring, 0)

    for k in range(4):
        slot = 2 * rem(x + k, 4) + 1 - core
        arrived(tok.at[slot], tok_recv.at[slot])

    def add_squares(s, total):
        values_in = tok[s].astype(jnp.float32)
        return total + jnp.sum(values_in * values_in, axis=1, keepdims=True)

    total_in = lax.fori_loop(0, 8, add_squares, jnp.zeros((ROWS, 1), jnp.float32))
    inv_in = lax.rsqrt(total_in / D + EPS)

    def normalize(s, _):
        gain = norm_gain[:, pl.ds(pl.multiple_of(s * 512, 512), 512)]
        rows = (tok[s].astype(jnp.float32) * inv_in * gain).astype(jnp.bfloat16)
        for j in range(8):
            nrm[s * 8 + j] = rows[:, j * UNIT : (j + 1) * UNIT]
        return 0

    lax.fori_loop(0, 8, normalize, 0)
    acc[...] = jnp.zeros_like(acc)

    def own_column(j, _):
        multiply(unit(offset(j), 0))
        return 0

    lax.fori_loop(0, 8, own_column, 0)

    def second_ring(d, plus, minus):
        def step(j, _):
            off = offset(j)
            low, high = unit(off, -d), unit(off, d)
            w_wait(low)
            if plus:
                pass_on(low, 0, 1)
            w_wait(high)
            if minus:
                pass_on(high, 0, -1)
            multiply(low)
            multiply(high)
            return 0

        return step

    lax.fori_loop(0, 8, second_ring(1, True, True), 0)
    lax.fori_loop(0, 8, second_ring(2, True, True), 0)
    lax.fori_loop(0, 4, second_ring(3, True, False), 0)
    lax.fori_loop(4, 8, second_ring(3, False, True), 0)

    def farthest(j, _):
        u = unit(offset(j), 4)
        w_wait(u)
        multiply(u)
        return 0

    lax.fori_loop(0, 8, farthest, 0)

    for m in range(2):
        keys[z, m] = acc[:, m * DK : (m + 1) * DK].astype(jnp.bfloat16)
        queries[y, m] = acc[:, 512 + m * DK : 512 + (m + 1) * DK].astype(jnp.bfloat16)
    values[z] = acc[:, 256:512].astype(jnp.bfloat16)

    def k_move(p, d):
        send(keys.at[p], keys.at[p], k_send, k_recv.at[p], at(along_z(d)))

    def v_move(p, d):
        send(values.at[p], values.at[p], v_send, v_recv.at[p], at(along_z(d)))

    def q_move(p, m, d):
        send(queries.at[p, m], queries.at[p, m], q_send, q_recv.at[p, m], at(along_y(d)))

    for d in (1, -1):
        k_move(z, d)
        for m in range(2):
            q_move(y, m, d)
        v_move(z, d)

    conv_in = acc[:, 768:896].astype(jnp.bfloat16).astype(jnp.float32)
    conv_c = acc[:, 1024:1152].astype(jnp.bfloat16).astype(jnp.float32)
    mixed[...] = (conv_c * conv_in).astype(jnp.bfloat16)
    send(mixed.at[pl.ds(176, 16)], halo, halo_send, halo_recv, at(after))

    for d in (1, 2, 3):
        low_z, high_z = rem(z - d + NZ, NZ), rem(z + d, NZ)
        low_y, high_y = rem(y - d + NY, NY), rem(y + d, NY)
        arrived(keys.at[low_z], k_recv.at[low_z])
        k_move(low_z, 1)
        arrived(keys.at[high_z], k_recv.at[high_z])
        if d < 3:
            k_move(high_z, -1)
        for m in range(2):
            arrived(queries.at[low_y, m], q_recv.at[low_y, m])
            if d < 4 - m:
                q_move(low_y, m, 1)
            arrived(queries.at[high_y, m], q_recv.at[high_y, m])
            if d < 3 + m:
                q_move(high_y, m, -1)
        arrived(values.at[low_z], v_recv.at[low_z])
        if d < 3:
            v_move(low_z, 1)
        arrived(values.at[high_z], v_recv.at[high_z])
        v_move(high_z, -1)

    arrived(halo, halo_recv)
    conv_b = acc[:, 896:1024].astype(jnp.bfloat16).astype(jnp.float32)
    mixed_now = mixed[...].astype(jnp.float32)
    earlier = jnp.where(sp > 0, halo[...].astype(jnp.float32), 0.0)
    padded = jnp.concatenate([earlier[8:16], mixed_now], axis=0)
    convolved = (
        conv_taps[0:1] * padded[6 : 6 + ROWS]
        + conv_taps[1:2] * padded[7 : 7 + ROWS]
        + conv_taps[2:3] * mixed_now
    )
    conv_out[...] = conv_b * convolved

    far_z, far_y = rem(z + 4, NZ), rem(y + 4, NY)
    for m in range(2):
        arrived(queries.at[far_y, m], q_recv.at[far_y, m])
    arrived(keys.at[far_z], k_recv.at[far_z])
    arrived(values.at[far_z], v_recv.at[far_z])

    scale = DK**-0.5 * LOG2E
    keys_here = NZ * ROWS
    spot = lax.broadcasted_iota(jnp.int32, (1, keys_here), 1)
    spot_z = div(spot, ROWS)
    key_block = spot_z * (NY * 3) + y * 3 + div(spot - spot_z * ROWS, UNIT)

    def partial(q_pos, m):
        all_keys = keys[:, m].reshape(keys_here, DK)
        all_values = values[...].reshape(keys_here, DV)
        reads, sums = [], []
        for b in range(3):
            limit = z * (NY * 3) + q_pos * 3 + b
            bias = jnp.where(key_block <= limit, 0.0, MASKED)
            scores = (
                lax.dot_general(
                    queries[q_pos, m, b * UNIT : (b + 1) * UNIT],
                    all_keys,
                    (((1,), (1,)), ((), ())),
                    preferred_element_type=jnp.float32,
                )
                + bias
            )
            top = jnp.max(scores, axis=1, keepdims=True)
            weights = jnp.exp2((scores - top) * scale)
            denom = jnp.sum(weights, axis=1, keepdims=True)
            product = jnp.dot(
                weights.astype(jnp.bfloat16), all_values, preferred_element_type=jnp.float32
            )
            reads.append(product / denom)
            level = top * scale + jnp.log2(denom)
            sums.append(jnp.where(y * 3 <= limit, level, MASKED))
        return jnp.concatenate(reads, axis=0), jnp.concatenate(sums, axis=0)

    def merge(reads, level, other, other_level):
        top = jnp.maximum(level, other_level)
        a = jnp.exp2(level - top)
        b = jnp.exp2(other_level - top)
        both = a + b
        inv = 1.0 / both
        return reads * (a * inv) + other * (b * inv), top + jnp.log2(both)

    def incoming(slot):
        arrived(in_slots.at[slot], o_recv.at[slot])
        arrived(in_rows.at[slot], l_recv.at[slot])

    def piece(t, _):
        i = div(t, 2)
        m = rem(t, 2)
        far = 4 - div(i + 1, 2)
        plus = jnp.where(jnp.logical_or(rem(i, 2) == 1, t == 0), 1, 0)
        q_pos = rem(y + far * (2 * plus - 1) + NY, NY)
        reads, level = partial(q_pos, m)
        has_other = jnp.logical_or(t >= 6, jnp.logical_or(t == 2, t == 5))

        @pl.when(has_other)
        def _():
            incoming(t)
            merged, merged_level = merge(
                reads,
                level,
                in_slots[t].astype(jnp.float32),
                to_column(in_rows[t, 0:1]),
            )
            out_slots[t] = merged.astype(jnp.bfloat16)
            out_rows[t] = to_row(merged_level)

        @pl.when(jnp.logical_not(has_other))
        def _():
            out_slots[t] = reads.astype(jnp.bfloat16)
            out_rows[t] = to_row(level)

        target = 2 * (10 - 2 * far - plus) + m
        device = at(along_y(2 * plus - 1))
        send(out_rows.at[t], in_rows.at[target], l_send, l_recv.at[target], device)
        send(out_slots.at[t], in_slots.at[target], o_send, o_recv.at[target], device)
        return 0

    lax.fori_loop(0, 14, piece, 0)

    def last_piece(m, _):
        reads, level = partial(y, m)
        for slot in (14 + m, 16 + m):
            incoming(slot)
            reads, level = merge(
                reads,
                level,
                in_slots[slot].astype(jnp.float32),
                to_column(in_rows[slot, 0:1]),
            )
        read[m] = reads
        return 0

    lax.fori_loop(0, 2, last_piece, 0)

    difference = read[0] - lam[0] * read[1]
    attn = (
        difference
        * lax.rsqrt(jnp.mean(difference * difference, axis=1, keepdims=True) + EPS)
        * head_scale[...]
    )
    conv = conv_out[...]
    both = jnp.sum(conv * conv, axis=1, keepdims=True) + jnp.sum(
        attn * attn, axis=1, keepdims=True
    )
    squares[mine] = to_row(both)
    for k in range(1, 8):
        other = rem(mine + k, 8)
        send(
            squares.at[mine],
            squares.at[mine],
            s_send,
            s_recv.at[mine],
            (sp, div(other, 2), rem(other, 2)),
        )
    for k in range(1, 8):
        other = rem(mine + k, 8)
        arrived(squares.at[other], s_recv.at[other])
    total = squares[0]
    for k in range(1, 8):
        total = total + squares[k]
    inv_rms = to_column(lax.rsqrt(total[0:1] / (CH + HEADS * DV) + EPS))
    conv_ref[...] = conv * inv_rms * gain_conv[...]
    attn_ref[...] = attn * inv_rms * gain_attn[...]

    arrived(tok.at[pl.ds(0, 7)], tok_send)
    arrived(wts.at[pl.ds(0, 63)], w_send)
    arrived(keys.at[pl.ds(0, 7)], k_send)
    arrived(values.at[pl.ds(0, 7)], v_send)
    arrived(queries.at[pl.ds(0, 7)], q_send)
    arrived(halo, halo_send)
    arrived(out_slots, o_send)
    arrived(out_rows, l_send)
    arrived(squares.at[pl.ds(0, 7)], s_send)


def local(
    tokens,
    norm_gain,
    w_conv_in,
    w_conv_b,
    w_conv_c,
    conv_taps,
    w_query,
    w_key,
    w_value,
    lam,
    head_scale,
    gain_conv,
    gain_attn,
):
    hbm = pl.BlockSpec(memory_space=pltpu.HBM)
    vmem = pl.BlockSpec(memory_space=pltpu.VMEM)
    smem = pl.BlockSpec(memory_space=pltpu.SMEM)
    bf16, f32 = jnp.bfloat16, jnp.float32
    dma = pltpu.SemaphoreType.DMA
    return pl.pallas_call(
        kernel,
        out_shape=(
            jax.ShapeDtypeStruct((ROWS, 128), f32),
            jax.ShapeDtypeStruct((ROWS, DV), f32),
        ),
        in_specs=[hbm] * 7 + [vmem, vmem, smem, vmem, vmem, vmem],
        out_specs=(vmem, vmem),
        scratch_shapes=[
            pltpu.VMEM((8, ROWS, 512), bf16),
            pltpu.VMEM((64, UNIT, COLS), bf16),
            pltpu.VMEM((64, ROWS, UNIT), bf16),
            pltpu.VMEM((ROWS, COLS), f32),
            pltpu.VMEM((NZ, 2, ROWS, DK), bf16),
            pltpu.VMEM((NZ, ROWS, DV), bf16),
            pltpu.VMEM((NY, 2, ROWS, DK), bf16),
            pltpu.VMEM((ROWS, 128), bf16),
            pltpu.VMEM((16, 128), bf16),
            pltpu.VMEM((14, ROWS, DV), bf16),
            pltpu.VMEM((14, 8, ROWS), f32),
            pltpu.VMEM((18, ROWS, DV), bf16),
            pltpu.VMEM((18, 8, ROWS), f32),
            pltpu.VMEM((8, 8, ROWS), f32),
            pltpu.VMEM((ROWS, 128), f32),
            pltpu.VMEM((2, ROWS, DV), f32),
            dma((7,)),
            dma,
            dma((8,)),
            dma,
            dma((64,)),
            dma,
            dma((NZ,)),
            dma,
            dma((NZ,)),
            dma,
            dma((NY, 2)),
            dma,
            dma,
            dma,
            dma((18,)),
            dma,
            dma((18,)),
            dma,
            dma((8,)),
        ],
        compiler_params=pltpu.CompilerParams(collective_id=0, has_side_effects=True),
    )(
        tokens,
        w_key,
        w_value,
        w_query,
        w_conv_in,
        w_conv_b,
        w_conv_c,
        norm_gain.reshape(1, D),
        conv_taps,
        lam,
        head_scale,
        gain_conv.reshape(1, -1),
        gain_attn.reshape(1, -1),
    )


def solution(mesh):
    in_specs = (
        P("sp", ("fs", "tp")),
        P(),
        P("sp", ("fs", "tp")),
        P("sp", ("fs", "tp")),
        P("sp", ("fs", "tp")),
        P(None, ("fs", "tp")),
        P("sp", ("fs", "tp")),
        P("sp", ("fs", "tp")),
        P("sp", ("fs", "tp")),
        P(("fs", "tp")),
        P(("fs", "tp"), None),
        P(("fs", "tp")),
        P(("fs", "tp")),
    )
    out_specs = (P("sp", ("fs", "tp")), P("sp", ("fs", "tp")))
    return jax.shard_map(local, mesh=mesh, in_specs=in_specs, out_specs=out_specs, check_vma=False)
```

time: 310 us -> 135 us (0.44)
  waiting for transfers between devices: 181 us -> 0 us
  Pallas kernels: 0 us -> 131 us
  blocking collectives: 39.3 us -> 0 us
  matrix products: 33.9 us -> 0 us
  local copies, waits for them, and re-layouts: 22.8 us -> 2.26 us
  other arithmetic: 14.2 us -> 0 us
  between operations: 15.1 us -> 1.3 us
  starting transfers between devices: 3.37 us -> 0 us
    all_gather x2 -> x0, waiting for transfers between devices: 181 us -> none  [the longest x1 104 us: in_one_piece(): lax.all_gather(both, axis, axis=dim, tiled=True)]
    pallas_call x0 -> x1, Pallas kernels: none -> 131 us  [local(): pl.pallas_call(kernel, out_shape=(jax.ShapeDtypeStruct((ROWS, 128), f32),...]
    all_to_all x2 -> x0, blocking collectives: 39.3 us -> none  [from_everyone(): return lax.all_to_all(copies, axis, split_axis=0, concat_axis=0, tiled=True)]
    dot_general x8 -> x0, matrix products: 33.9 us -> none  [the longest x6 12.5 us: absorb_rows(): jnp.dot(normed, piece, preferred_element_type=jnp.float32)]
    another operation x1 -> x0, local copies, waits for them, and re-layouts: 9.72 us -> none
    reduce_sum x5 -> x0, other arithmetic: 9.63 us -> none  [the longest x1 8.9 us: absorb_keys(): row_total = jnp.sum(weights, axis=-1)]
    slice x2 -> x0, local copies, waits for them, and re-layouts: 6.43 us -> none  [the longest x1 6.42 us: in_one_piece(): piece = result[..., at:at + column.shape[along]]]
    ppermute x1 -> x0, starting transfers between devices: 3.29 us -> none  [from_behind(): return lax.ppermute(block, axis, route)]
  transfers between devices with their start and end apart: 3 -> 0, of which waited for: 2 -> 0; matrix products, arithmetic and copies ran while one was open for 4% -> 0% of each run, Pallas kernels for 0% -> 0%
where the time goes in v1:
time: 135 us
  Pallas kernels  131 us (97%)
  local copies, waits for them, and re-layouts  2.26 us (2%)
    pallas_call x1, Pallas kernels, local(): pl.pallas_call(kernel, out_shape=(jax.ShapeDtypeStruct((ROWS, 128), f32),...  131 us

profile of v1, /device:TPU:1, one launch (start us, length us, event | category | flops | bytes accessed | tf_op | source)
XLA Modules:
  0.0 134.8 jit_solution(2567046260545449965)
XLA Ops:
  1.3 131.3 %shard_map.140 = (f32[192,128]{1,0:T(8,128)}, f32[192,256]{1,0:T(8,128)}) custom-call(bf16[192,512]{1,0:T(8,128)(2,1)} %tokens.1, bf16[64,256]{1,0:T(8,128)(2,1)} %w_key.1, bf16[64,256]{1,0:T(8,128)(2,1)} %w_value.1, bf16[64,256]{1,0:T(8,128)(2,1)} %w_query.1, bf16[64,128]{1,0:T(8,128)(2,1)} %w_conv_in.1, bf16[64,128]{1,0:T(8,128)(2,1)} %w_conv_b.1, ...), custom_call_target="tpu_custom_call" | custom-call | tf_op jit(solution)/shard_map/pallas_call | solution.py:499
  132.6 0.0 copy-start
  132.6 1.6 %copy.18 = f32[192,128]{1,0:T(8,128)} copy(f32[192,128]{1,0:T(8,128)} %get-tuple-element.4) | data formatting | bytes 196608
  134.2 0.0 copy-done
  134.2 0.7 copy.19
Async XLA Ops:
  132.6 1.6 %copy-start = (f32[192,256]{1,0:T(8,128)S(1)}, f32[192,256]{1,0:T(8,128)}, u32[]{:S(2)}) copy-start(f32[192,256]{1,0:T(8,128)} %get-tuple-element.5) | copy-start | bytes 589828

commit v2 on v1

v2 whole, which is shorter than its diff:
```python
import functools
import math

import jax
import jax.numpy as jnp
from jax import lax
from jax.experimental import pallas as pl
from jax.experimental.pallas import tpu as pltpu
from jax.sharding import PartitionSpec as P

NY = 8
NZ = 8
D = 4096
CH = 1024
HEADS = 8
DK = 128
DV = 256
ROWS = 192
UNIT = 64
EPS = 1e-06
MASKED = -1e30
LOG2E = 1.4426950408889634
LN2 = 0.6931471805599453
MESH = pl.DeviceIdType.MESH

GROUP = 384


def rem(a, n):
    return lax.rem(a, jnp.int32(n))


def div(a, n):
    return lax.div(a, jnp.int32(n))


def to_row(column):
    wide = jnp.broadcast_to(column, (ROWS, 128))
    return jnp.transpose(wide)[0:8]


def to_column(row):
    tall = jnp.broadcast_to(row, (128, ROWS))
    return jnp.transpose(tall)[:, 0:1]


def kernel(
    tokens,
    w_key,
    w_value,
    w_query,
    w_conv_in,
    w_conv_b,
    w_conv_c,
    norm_gain,
    conv_taps,
    lam,
    head_scale,
    gain_conv,
    gain_attn,
    conv_ref,
    attn_ref,
    tok,
    wts,
    nrm,
    acc,
    keys,
    values,
    queries,
    mixed,
    halo,
    out_slots,
    out_rows,
    in_slots,
    in_rows,
    squares,
    conv_out,
    turned,
    held_reads,
    held_levels,
    local_sem,
    tok_send,
    tok_recv,
    far_recv,
    w_send,
    w_recv,
    k_send,
    k_recv,
    v_send,
    v_recv,
    q_send,
    q_recv,
    halo_send,
    halo_recv,
    o_send,
    o_recv,
    l_send,
    l_recv,
    s_send,
    s_recv,
):
    sp = lax.axis_index("sp")
    x = lax.axis_index("fs")
    core = lax.axis_index("tp")
    y = rem(sp, NY)
    z = div(sp, NY)
    mine = 2 * x + core

    def at(s, f=x, t=core):
        return (s, f, t)

    def along_y(d):
        return sp + rem(y + d + NY, NY) - y

    def along_z(d):
        return sp + (rem(z + d + NZ, NZ) - z) * NY

    def send(src, dst, send_sem, recv_sem, device):
        pltpu.make_async_remote_copy(
            src_ref=src,
            dst_ref=dst,
            send_sem=send_sem,
            recv_sem=recv_sem,
            device_id=device,
            device_id_type=MESH,
        ).start()

    def arrived(ref, sem):
        pltpu.make_async_copy(ref, ref, sem).wait()

    own = [
        pltpu.make_async_copy(tokens, tok.at[mine], local_sem.at[0]),
    ]
    group_parts = (
        (w_key, 0, 0, 0, 256),
        (w_query, 0, 0, 256, 128),
        (w_value, 0, 1, 0, 256),
        (w_query, 128, 1, 256, 128),
        (w_conv_in, 0, 2, 0, 128),
        (w_conv_b, 0, 2, 128, 128),
        (w_conv_c, 0, 2, 256, 128),
    )
    home = y * (1 + 7 * core) + z * (8 - 7 * core)
    for k, (w, start, g, column, width) in enumerate(group_parts):
        own.append(
            pltpu.make_async_copy(
                w.at[:, pl.ds(start, width)],
                wts.at[g, home, :, pl.ds(column, width)],
                local_sem.at[1 + k],
            )
        )
    for copy in own:
        copy.start()

    barrier = pltpu.get_barrier_semaphore()

    def greet(device):
        pl.semaphore_signal(barrier, inc=1, device_id=device, device_id_type=MESH)

    for d in (1, -1):
        greet(at(along_y(d)))
        greet(at(along_z(d)))
    for k in range(1, 8):
        other = rem(mine + k, 8)
        greet((sp, div(other, 2), rem(other, 2)))
    before = rem(sp + NY * NZ - 1, NY * NZ)
    after = rem(sp + 1, NY * NZ)
    greet(at(before))
    for copy in own:
        copy.wait()
    pl.semaphore_wait(barrier, 12)

    def slot_at(k):
        return 2 * rem(x + k + 4, 4) + core

    def tok_to(k, slot, rows, sem):
        part = tok.at[slot, rows]
        send(part, part, tok_send, sem, at(sp, rem(x + k + 4, 4)))

    def to_partner(slot):
        send(tok.at[slot], tok.at[slot], tok_send, tok_recv.at[slot], at(sp, x, 1 - core))

    upper, lower = pl.ds(0, ROWS // 2), pl.ds(ROWS // 2, ROWS // 2)
    for k in (1, -1):
        tok_to(k, mine, pl.ds(0, ROWS), tok_recv.at[mine])
    to_partner(mine)

    stride1 = 1 + 7 * core
    stride2 = 8 - 7 * core
    pos1 = rem(lax.div(sp, stride1), 8)
    pos2 = rem(lax.div(sp, stride2), 8)

    def place(d1, d2):
        return rem(pos2 + d2 + 8, 8) * 8 + rem(pos1 + d1 + 8, 8)

    def device(d1, d2):
        return at(rem(pos1 + d1 + 8, 8) * stride1 + rem(pos2 + d2 + 8, 8) * stride2)

    def pass_on(g, u, d1, d2):
        send(wts.at[g, u], wts.at[g, u], w_send.at[g], w_recv.at[g, u], device(d1, d2))

    def w_wait(g, u):
        arrived(wts.at[g, u], w_recv.at[g, u])

    def offset(j):
        return div(j + 1, 2) * (1 - 2 * rem(j, 2))

    def loop(first, last, *steps):
        def body(j, _):
            for step in steps:
                step(j)
            return 0

        lax.fori_loop(first, last, body, 0)

    def first_ring(g, lag=0, onward=True):
        def step(i):
            j = i - lag
            off = offset(j)
            u = place(off, 0)

            @pl.when(j > 0)
            def _():
                w_wait(g, u)

            @pl.when(jnp.logical_and(off <= 0, off > -4))
            def _():
                pass_on(g, u, 1, 0)

            @pl.when(jnp.logical_and(off >= 0, off < 3))
            def _():
                pass_on(g, u, -1, 0)

            if onward:
                across(g)(j)

        return step

    def across(g):
        def step(j):
            u = place(offset(j), 0)
            pass_on(g, u, 0, 1)
            pass_on(g, u, 0, -1)

        return step

    def second_ring(g, d, lag=0):
        def step(i):
            j = i - lag
            off = offset(j)
            if d == 4:
                w_wait(g, place(off, 4))
                return
            low, high = place(off, -d), place(off, d)
            w_wait(g, low)
            if d < 3:
                pass_on(g, low, 0, 1)
            else:

                @pl.when(j < 4)
                def _():
                    pass_on(g, low, 0, 1)

            w_wait(g, high)
            if d < 3:
                pass_on(g, high, 0, -1)
            else:

                @pl.when(j >= 4)
                def _():
                    pass_on(g, high, 0, -1)

        return step

    def multiply(*distances):
        for d in distances:
            p = rem(pos2 + d + 8, 8)
            for g in range(2):
                block = wts[g, pl.ds(p * 8, 8)].reshape(8 * UNIT, GROUP)
                acc[g] += jnp.dot(nrm[p], block, preferred_element_type=jnp.float32)

    with jax.named_scope("ring1a"):
        loop(0, 3, first_ring(0), first_ring(1))
    with jax.named_scope("tokpass"):
        for k, rows in ((-1, upper), (1, lower)):
            slot = slot_at(k)
            arrived(tok.at[slot], tok_recv.at[slot])
            tok_to(-k, slot, rows, far_recv.at[0 if k < 0 else 1])
            to_partner(slot)
    with jax.named_scope("ring1b"):
        loop(
            3,
            8,
            first_ring(0),
            first_ring(1),
            second_ring(0, 1, 3),
            second_ring(1, 1, 3),
            first_ring(2, 3, False),
        )

    with jax.named_scope("tokpass2"):
        far = slot_at(2)
        arrived(tok.at[far, upper], far_recv.at[0])
        arrived(tok.at[far, lower], far_recv.at[1])
        to_partner(far)
    with jax.named_scope("ring1c"):
        loop(5, 8, second_ring(0, 1), second_ring(1, 1), first_ring(2, 0, False))
    with jax.named_scope("norm"):
        for k in range(4):
            slot = 2 * rem(x + k, 4) + 1 - core
            arrived(tok.at[slot], tok_recv.at[slot])

        def add_squares(s, total):
            values_in = tok[s].astype(jnp.float32)
            return total + jnp.sum(values_in * values_in, axis=1, keepdims=True)

        total_in = lax.fori_loop(0, 8, add_squares, jnp.zeros((ROWS, 1), jnp.float32))
        inv_in = lax.rsqrt(total_in / D + EPS)

        def normed(s):
            gain = norm_gain[:, s * 512 : (s + 1) * 512]
            return (tok[s].astype(jnp.float32) * inv_in * gain).astype(jnp.bfloat16)

        @pl.when(core == 0)
        def _():
            for s in range(8):
                nrm[s] = normed(s)

        @pl.when(core == 1)
        def _():
            for s in range(8):
                rows = normed(s)
                for j in range(8):
                    nrm[j, :, s * UNIT : (s + 1) * UNIT] = rows[:, j * UNIT : (j + 1) * UNIT]

        acc[...] = jnp.zeros_like(acc)
        multiply(0, -1, 1)
    with jax.named_scope("d2"):
        loop(0, 8, second_ring(0, 2), second_ring(1, 2))
        multiply(-2, 2)
    with jax.named_scope("d3"):
        loop(0, 8, second_ring(0, 3), second_ring(1, 3))
        loop(0, 8, across(2))
        multiply(-3, 3)
    with jax.named_scope("d4"):
        loop(0, 8, second_ring(0, 4), second_ring(1, 4))
        multiply(4)

    with jax.named_scope("qkv"):
        for m in range(2):
            keys[z, m] = acc[0, :, m * DK : (m + 1) * DK].astype(jnp.bfloat16)
            queries[y, m] = acc[m, :, 256:384].astype(jnp.bfloat16)
        values[z] = acc[1, :, 0:256].astype(jnp.bfloat16)

    def k_move(p, d):
        send(keys.at[p], keys.at[p], k_send, k_recv.at[p], at(along_z(d)))

    def v_move(p, d):
        send(values.at[p], values.at[p], v_send, v_recv.at[p], at(along_z(d)))

    def q_move(p, m, d):
        send(queries.at[p, m], queries.at[p, m], q_send, q_recv.at[p, m], at(along_y(d)))

    for d in (1, -1):
        k_move(z, d)
        for m in range(2):
            q_move(y, m, d)
        v_move(z, d)

    for d in (1, 2, 3):
        with jax.named_scope(f"qkv{d}"):
            low_z, high_z = rem(z - d + NZ, NZ), rem(z + d, NZ)
            low_y, high_y = rem(y - d + NY, NY), rem(y + d, NY)
            arrived(keys.at[low_z], k_recv.at[low_z])
            k_move(low_z, 1)
            arrived(keys.at[high_z], k_recv.at[high_z])
            if d < 3:
                k_move(high_z, -1)
            for m in range(2):
                arrived(queries.at[low_y, m], q_recv.at[low_y, m])
                if d < 4 - m:
                    q_move(low_y, m, 1)
                arrived(queries.at[high_y, m], q_recv.at[high_y, m])
                if d < 3 + m:
                    q_move(high_y, m, -1)
            arrived(values.at[low_z], v_recv.at[low_z])
            if d < 3:
                v_move(low_z, 1)
            arrived(values.at[high_z], v_recv.at[high_z])
            v_move(high_z, -1)
        with jax.named_scope(f"w{d}"):
            if d == 1:
                loop(0, 4, second_ring(2, 1))
            if d == 2:
                loop(4, 8, second_ring(2, 1))
            if d == 3:
                loop(0, 4, second_ring(2, 2))

    with jax.named_scope("qkv4"):
        far_z, far_y = rem(z + 4, NZ), rem(y + 4, NY)
        for m in range(2):
            arrived(queries.at[far_y, m], q_recv.at[far_y, m])
        arrived(keys.at[far_z], k_recv.at[far_z])
        arrived(values.at[far_z], v_recv.at[far_z])

    keys_here = NZ * ROWS
    with jax.named_scope("turn"):
        for m in range(2):
            turned[m] = jnp.transpose(keys[:, m].reshape(keys_here, DK))

    def convolution_input():
        every = wts[2].reshape(D, GROUP)
        acc[2] = jnp.zeros((ROWS, GROUP), jnp.float32)
        for p in range(8):
            acc[2] += jnp.dot(
                nrm[p],
                every[p * 512 : (p + 1) * 512],
                preferred_element_type=jnp.float32,
            )
        conv_in = acc[2, :, 0:128].astype(jnp.bfloat16).astype(jnp.float32)
        conv_c = acc[2, :, 256:384].astype(jnp.bfloat16).astype(jnp.float32)
        mixed[...] = (conv_c * conv_in).astype(jnp.bfloat16)
        send(mixed.at[pl.ds(176, 16)], halo, halo_send, halo_recv, at(after))

    def convolution():
        arrived(halo, halo_recv)
        conv_b = acc[2, :, 128:256].astype(jnp.bfloat16).astype(jnp.float32)
        mixed_now = mixed[...].astype(jnp.float32)
        earlier = jnp.where(sp > 0, halo[...].astype(jnp.float32), 0.0)
        padded = jnp.concatenate([earlier[8:16], mixed_now], axis=0)
        convolved = (
            conv_taps[0:1] * padded[6 : 6 + ROWS]
            + conv_taps[1:2] * padded[7 : 7 + ROWS]
            + conv_taps[2:3] * mixed_now
        )
        conv_out[...] = conv_b * convolved

    scale = DK**-0.5 * LOG2E
    spot = lax.broadcasted_iota(jnp.int32, (1, keys_here), 1)
    spot_z = div(spot, ROWS)
    key_block = spot_z * (NY * 3) + y * 3 + div(spot - spot_z * ROWS, UNIT)

    def partials(q_pos):
        first = z * (NY * 3) + q_pos * 3
        biases = [jnp.where(key_block <= first + b, 0.0, MASKED) for b in range(3)]
        weights, denoms, levels = [], [], []
        for m in range(2):
            scores = jnp.dot(
                queries[q_pos, m], turned[m], preferred_element_type=jnp.float32
            )
            for b in range(3):
                part = scores[b * UNIT : (b + 1) * UNIT] + biases[b]
                top = jnp.max(part, axis=1, keepdims=True)
                shares = jnp.exp2((part - top) * scale)
                denom = jnp.sum(shares, axis=1, keepdims=True)
                weights.append(shares.astype(jnp.bfloat16))
                denoms.append(denom)
                level = top * scale + jnp.log2(denom)
                levels.append(jnp.where(y * 3 <= first + b, level, MASKED))
        product = jnp.dot(
            jnp.concatenate(weights, axis=0),
            values[...].reshape(keys_here, DV),
            preferred_element_type=jnp.float32,
        ) * (1.0 / jnp.concatenate(denoms, axis=0))
        level = jnp.concatenate(levels, axis=0)
        return [(product[m * ROWS : (m + 1) * ROWS], level[m * ROWS : (m + 1) * ROWS]) for m in range(2)]

    def merge(reads, level, other, other_level):
        top = jnp.maximum(level, other_level)
        a = jnp.exp2(level - top)
        b = jnp.exp2(other_level - top)
        both = a + b
        inv = 1.0 / both
        return reads * (a * inv) + other * (b * inv), top + jnp.log2(both)

    def incoming(slot):
        arrived(in_slots.at[slot], o_recv.at[slot])
        arrived(in_rows.at[slot], l_recv.at[slot])

    def pieces(i, _):
        hops = 4 - div(i + 1, 2)
        q_pos = rem(y + hops * (2 * rem(i, 2) - 1) + NY, NY)
        with jax.named_scope("partial"):
            both = partials(q_pos)

        def post(t, m, reads, level):
            out_slots[t] = reads.astype(jnp.bfloat16)
            out_rows[t] = to_row(level)
            step = div(t, 2)
            hop = 4 - div(step + 1, 2)
            plus = jnp.where(step == 0, 1 - m, rem(step, 2))
            target = 2 * (10 - 2 * hop - plus) + m
            to = at(along_y(2 * plus - 1))
            send(out_rows.at[t], in_rows.at[target], l_send, l_recv.at[target], to)
            send(out_slots.at[t], in_slots.at[target], o_send, o_recv.at[target], to)

        def join(t, m, reads, level):
            with jax.named_scope("incoming"):
                incoming(t)
            post(
                t,
                m,
                *merge(reads, level, in_slots[t].astype(jnp.float32), to_column(in_rows[t, 0:1])),
            )

        for m in range(2):
            reads, level = both[m]

            @pl.when(i >= 3)
            def _():
                join(2 * i + m, m, reads, level)

            @pl.when(i == 1 + m)
            def _():
                held_reads[m] = reads
                held_levels[m] = jnp.broadcast_to(level, (ROWS, 128))

            @pl.when(jnp.logical_and(i < 3, i != 1 + m))
            def _():
                post(2 * i + m, m, reads, level)

        @pl.when(i == 2)
        def _():
            join(2, 0, held_reads[0], held_levels[0, :, 0:1])
            join(5, 1, held_reads[1], held_levels[1, :, 0:1])

        with jax.named_scope("weights"):

            @pl.when(i == 0)
            def _():
                loop(4, 8, second_ring(2, 2))

            @pl.when(i == 1)
            def _():
                loop(0, 4, second_ring(2, 3))

            @pl.when(i == 2)
            def _():
                loop(4, 8, second_ring(2, 3))

            @pl.when(i == 3)
            def _():
                loop(0, 4, second_ring(2, 4))

            @pl.when(i == 4)
            def _():
                loop(4, 8, second_ring(2, 4))

            @pl.when(i == 5)
            def _():
                convolution_input()

        return 0

    with jax.named_scope("pieces"):
        lax.fori_loop(0, 7, pieces, 0)

    with jax.named_scope("last"):
        own_parts = partials(y)
        read = []
        for m in range(2):
            reads, level = own_parts[m]
            for slot in (14 + m, 16 + m):
                with jax.named_scope("incoming"):
                    incoming(slot)
                reads, level = merge(
                    reads,
                    level,
                    in_slots[slot].astype(jnp.float32),
                    to_column(in_rows[slot, 0:1]),
                )
            read.append(reads)

    def finish():
        arrived(tok.at[pl.ds(0, 7)], tok_send)
        for g in range(3):
            arrived(wts.at[g, pl.ds(0, 63)], w_send.at[g])
        arrived(keys.at[pl.ds(0, 7)], k_send)
        arrived(values.at[pl.ds(0, 7)], v_send)
        arrived(queries.at[pl.ds(0, 7)], q_send)
        arrived(halo, halo_send)
        arrived(out_slots, o_send)
        arrived(out_rows, l_send)
        arrived(squares.at[pl.ds(0, 7)], s_send)

    with jax.named_scope("conv"):
        convolution()
    with jax.named_scope("sum"):
        difference = read[0] - lam[0] * read[1]
        attn = (
            difference
            * lax.rsqrt(jnp.mean(difference * difference, axis=1, keepdims=True) + EPS)
            * head_scale[...]
        )
        conv = conv_out[...]
        both = jnp.sum(conv * conv, axis=1, keepdims=True) + jnp.sum(
            attn * attn, axis=1, keepdims=True
        )
        squares[mine] = to_row(both)
        for k in range(1, 8):
            other = rem(mine + k, 8)
            send(
                squares.at[mine],
                squares.at[mine],
                s_send,
                s_recv.at[mine],
                (sp, div(other, 2), rem(other, 2)),
            )
    with jax.named_scope("exchange"):
        for k in range(1, 8):
            other = rem(mine + k, 8)
            arrived(squares.at[other], s_recv.at[other])
    with jax.named_scope("out"):
        total = squares[0]
        for k in range(1, 8):
            total = total + squares[k]
        inv_rms = to_column(lax.rsqrt(total[0:1] / (CH + HEADS * DV) + EPS))
        conv_ref[...] = conv * inv_rms * gain_conv[...]
        attn_ref[...] = attn * inv_rms * gain_attn[...]

    with jax.named_scope("drain"):
        finish()


def local(
    tokens,
    norm_gain,
    w_conv_in,
    w_conv_b,
    w_conv_c,
    conv_taps,
    w_query,
    w_key,
    w_value,
    lam,
    head_scale,
    gain_conv,
    gain_attn,
):
    hbm = pl.BlockSpec(memory_space=pltpu.HBM)
    vmem = pl.BlockSpec(memory_space=pltpu.VMEM)
    smem = pl.BlockSpec(memory_space=pltpu.SMEM)
    bf16, f32 = jnp.bfloat16, jnp.float32
    dma = pltpu.SemaphoreType.DMA
    return pl.pallas_call(
        kernel,
        out_shape=(
            jax.ShapeDtypeStruct((ROWS, 128), f32),
            jax.ShapeDtypeStruct((ROWS, DV), f32),
        ),
        in_specs=[hbm] * 7 + [vmem, vmem, smem, vmem, vmem, vmem],
        out_specs=(vmem, vmem),
        scratch_shapes=[
            pltpu.VMEM((8, ROWS, 512), bf16),
            pltpu.VMEM((3, 64, UNIT, GROUP), bf16),
            pltpu.VMEM((8, ROWS, 512), bf16),
            pltpu.VMEM((3, ROWS, GROUP), f32),
            pltpu.VMEM((NZ, 2, ROWS, DK), bf16),
            pltpu.VMEM((NZ, ROWS, DV), bf16),
            pltpu.VMEM((NY, 2, ROWS, DK), bf16),
            pltpu.VMEM((ROWS, 128), bf16),
            pltpu.VMEM((16, 128), bf16),
            pltpu.VMEM((14, ROWS, DV), bf16),
            pltpu.VMEM((14, 8, ROWS), f32),
            pltpu.VMEM((18, ROWS, DV), bf16),
            pltpu.VMEM((18, 8, ROWS), f32),
            pltpu.VMEM((8, 8, ROWS), f32),
            pltpu.VMEM((ROWS, 128), f32),
            pltpu.VMEM((2, DK, NZ * ROWS), bf16),
            pltpu.VMEM((2, ROWS, DV), f32),
            pltpu.VMEM((2, ROWS, 128), f32),
            dma((8,)),
            dma,
            dma((8,)),
            dma((2,)),
            dma((3,)),
            dma((3, 64)),
            dma,
            dma((NZ,)),
            dma,
            dma((NZ,)),
            dma,
            dma((NY, 2)),
            dma,
            dma,
            dma,
            dma((18,)),
            dma,
            dma((18,)),
            dma,
            dma((8,)),
        ],
        compiler_params=pltpu.CompilerParams(collective_id=0, has_side_effects=True),
    )(
        tokens,
        w_key,
        w_value,
        w_query,
        w_conv_in,
        w_conv_b,
        w_conv_c,
        norm_gain.reshape(1, D),
        conv_taps,
        lam,
        head_scale,
        gain_conv.reshape(1, -1),
        gain_attn.reshape(1, -1),
    )


def solution(mesh):
    in_specs = (
        P("sp", ("fs", "tp")),
        P(),
        P("sp", ("fs", "tp")),
        P("sp", ("fs", "tp")),
        P("sp", ("fs", "tp")),
        P(None, ("fs", "tp")),
        P("sp", ("fs", "tp")),
        P("sp", ("fs", "tp")),
        P("sp", ("fs", "tp")),
        P(("fs", "tp")),
        P(("fs", "tp"), None),
        P(("fs", "tp")),
        P(("fs", "tp")),
    )
    out_specs = (P("sp", ("fs", "tp")), P("sp", ("fs", "tp")))
    return jax.shard_map(local, mesh=mesh, in_specs=in_specs, out_specs=out_specs, check_vma=False)
```

time: 135 us -> 117 us (0.87)
  Pallas kernels: 131 us -> 113 us
    pallas_call x1, Pallas kernels: 131 us -> 113 us  [local(): pl.pallas_call(kernel, out_shape=(jax.ShapeDtypeStruct((ROWS, 128), f32),...]
where the time goes in v2:
time: 117 us; the launch traced here: 116 us
  Pallas kernels  113 us (97%)
  local copies, waits for them, and re-layouts  2.26 us (2%)
  between operations  1.3 us (1%)
    pallas_call x1, Pallas kernels, local(): pl.pallas_call(kernel, out_shape=(jax.ShapeDtypeStruct((ROWS, 128), f32),...  113 us

profile of v2, /device:TPU:1, one launch (start us, length us, event | category | flops | bytes accessed | tf_op | source)
XLA Modules:
  0.0 116.4 jit_solution(6319254631036038124)
XLA Ops:
  1.3 112.9 %shard_map.140 = (f32[192,128]{1,0:T(8,128)}, f32[192,256]{1,0:T(8,128)}) custom-call(bf16[192,512]{1,0:T(8,128)(2,1)} %tokens.1, bf16[64,256]{1,0:T(8,128)(2,1)} %w_key.1, bf16[64,256]{1,0:T(8,128)(2,1)} %w_value.1, bf16[64,256]{1,0:T(8,128)(2,1)} %w_query.1, bf16[64,128]{1,0:T(8,128)(2,1)} %w_conv_in.1, bf16[64,128]{1,0:T(8,128)(2,1)} %w_conv_b.1, ...), custom_call_target="tpu_custom_call" | custom-call | tf_op jit(solution)/shard_map/pallas_call | solution.py:645
  114.2 0.0 copy-start
  114.2 1.6 %copy.18 = f32[192,128]{1,0:T(8,128)} copy(f32[192,128]{1,0:T(8,128)} %get-tuple-element.4) | data formatting | bytes 196608
  115.7 0.0 copy-done
  115.7 0.7 copy.19
Async XLA Ops:
  114.2 1.6 %copy-start = (f32[192,256]{1,0:T(8,128)S(1)}, f32[192,256]{1,0:T(8,128)}, u32[]{:S(2)}) copy-start(f32[192,256]{1,0:T(8,128)} %get-tuple-element.5) | copy-start | bytes 589828
